TPU v7x, 32 devices: a whole 2x2x4 slice. The times are simulated.
32 devices in a mesh: sp: 8 (over z, x), tp: 4 (over y, core).
Axes of the slice: x: 2, y: 2, z: 4, core: 2. Of those that a mesh axis runs over, the one named last changes fastest.
Arguments:
- mixer_out: bfloat16 [1024, 2048], P('sp'), may hold values from -6 to 6
- out_grad: bfloat16 [1024, 2048], P('sp'), may hold values from -2 to 2
- route_ids: int32 [1024, 2], P('sp'), may hold values from 0 to 7, all different within a row; in each aligned block of 128 rows (0 to 127, 128 to 255, ...) at most 64 rows name the same one
- route_weights: float32 [1024, 2], P('sp'), may hold values from 0.2 to 1.2
- gate_branch: bfloat16 [1024, 2048], P('sp', 'tp'), may hold values from -4 to 4
- states: float32 [1024, 2048], P('sp', 'tp'), may hold values from -6 to 6
- decay: float32 [1024, 2048], P('sp', 'tp'), may hold values from 0 to 1
- w_proj: bfloat16 [2048, 2048], P(None, 'tp'), may hold values from -0.125 to 0.125
- w_gate: bfloat16 [8, 2048, 2048], P('sp', 'tp'), may hold values from -0.125 to 0.125
- w_up: bfloat16 [8, 2048, 2048], P('sp', 'tp'), may hold values from -0.125 to 0.125
- w_down: bfloat16 [8, 2048, 2048], P('sp', 'tp'), may hold values from -0.125 to 0.125
Outputs:
- grad_w_gate: bfloat16 [8, 2048, 2048], P('sp', 'tp')
- grad_w_up: bfloat16 [8, 2048, 2048], P('sp', 'tp')
- grad_w_down: bfloat16 [8, 2048, 2048], P('sp', 'tp')
- grad_w_proj: float32 [2048, 2048], P('sp', 'tp')
- grad_branch: bfloat16 [1024, 2048], P('sp', 'tp')
- grad_drive: float32 [1024, 2048], P('sp', 'tp')
- grad_decay: float32 [1024, 2048], P('sp', 'tp')
Inputs may be any that keep to these rules, and one draw needn't show every extreme that they name: `route_ids`: each row names 2 different experts. In the rows of one index of sp no expert is named more than 64 times, a bound that some block reaches.
All inputs are finite; a program needn't handle non-finite values.
Results may differ from a plain program's by a relative error of at most 0.02.
Values may be sent and summed in bfloat16 or wider, within the bound.
A program may use at most 64 MiB of HBM per device.

v0:
```python
import jax
import jax.numpy as jnp
from jax import lax
from jax.sharding import PartitionSpec as P


def entering(value, axis, join, neutral):
    count, mine = (lax.axis_size(axis), lax.axis_index(axis))
    pieces = jax.tree.map(lambda part: lax.all_gather(part, axis), value)
    pieces = jax.tree.map(lambda part: part[::-1], pieces)
    mine = count - 1 - mine
    so_far = jax.tree.map(
        lambda part, zero: jnp.full_like(part, 0) + jnp.asarray(zero, part.dtype), value, neutral
    )

    def lap(position, so_far):
        longer = join(so_far, jax.tree.map(lambda part: part[position], pieces))
        return jax.tree.map(lambda new, old: jnp.where(position < mine, new, old), longer, so_far)

    return lax.fori_loop(0, count - 1, lap, so_far)


def shifted(block, axis, distance):
    devices = range(lax.axis_size(axis))
    route = [(i - distance, i) for i in devices if i - distance in devices]
    return lax.ppermute(block, axis, route)


def linear_combine(earlier, later):
    return (earlier[0] * later[0], later[0] * earlier[1] + later[1])


def chain_combine(earlier, later):
    return (later[0] * earlier[0], later[1] + later[0] * earlier[1])


def expert_grads(inputs, cotangents, w_gate, w_up, w_down):
    gate_pre = jnp.einsum("esd,efd->esf", inputs, w_gate, preferred_element_type=jnp.float32)
    up_pre = jnp.einsum("esd,efd->esf", inputs, w_up, preferred_element_type=jnp.float32)
    sigmoid_gate = jax.nn.sigmoid(gate_pre)
    silu_gate = gate_pre * sigmoid_gate
    hidden = (silu_gate * up_pre).astype(jnp.bfloat16)
    hidden_grad = jnp.einsum("esd,efd->esf", cotangents, w_down, preferred_element_type=jnp.float32)
    up_grad = (hidden_grad * silu_gate).astype(jnp.bfloat16)
    gate_grad = (
        hidden_grad * up_pre * sigmoid_gate * (1.0 + gate_pre * (1.0 - sigmoid_gate))
    ).astype(jnp.bfloat16)
    grad_gate = jnp.einsum(
        "esf,esd->efd", gate_grad, inputs, preferred_element_type=jnp.float32
    ).astype(jnp.bfloat16)
    grad_up = jnp.einsum(
        "esf,esd->efd", up_grad, inputs, preferred_element_type=jnp.float32
    ).astype(jnp.bfloat16)
    grad_down = jnp.einsum(
        "esf,esd->efd", hidden, cotangents, preferred_element_type=jnp.float32
    ).astype(jnp.bfloat16)
    partial_value = jnp.einsum(
        "esf,efd->esd", gate_grad, w_gate, preferred_element_type=jnp.float32
    )
    partial_value = partial_value + jnp.einsum(
        "esf,efd->esd", up_grad, w_up, preferred_element_type=jnp.float32
    )
    return (grad_gate, grad_up, grad_down, partial_value.astype(jnp.bfloat16))


def local(
    mixer_out,
    out_grad,
    route_ids,
    route_weights,
    gate_branch,
    states,
    decay,
    w_proj,
    w_gate,
    w_up,
    w_down,
):
    tok_rows, model_width = mixer_out.shape
    top_count = route_ids.shape[1]
    local_experts = w_gate.shape[0]
    sp_size = lax.axis_size("sp")
    tp_size = lax.axis_size("tp")
    experts = local_experts * sp_size
    capacity = 2 * top_count * tok_rows // experts
    routes = tok_rows * top_count
    flat_ids = route_ids.reshape(-1)
    onehot = (flat_ids[:, None] == jnp.arange(experts, dtype=jnp.int32)[None, :]).astype(jnp.int32)
    position = jnp.sum(jnp.cumsum(onehot, axis=0) * onehot, axis=1) - 1
    bucket = flat_ids % local_experts * sp_size + flat_ids // local_experts
    slot_index = bucket * capacity + position
    source = (
        jnp.full((experts * capacity,), routes, jnp.int32)
        .at[slot_index]
        .set(jnp.arange(routes, dtype=jnp.int32))
    )
    scaled = (route_weights[:, :, None] * out_grad[:, None, :].astype(jnp.float32)).astype(
        jnp.bfloat16
    )
    scaled_pad = jnp.concatenate(
        [scaled.reshape(routes, model_width), jnp.zeros((1, model_width), jnp.bfloat16)], axis=0
    )
    token_pad = jnp.concatenate([mixer_out, jnp.zeros((1, model_width), jnp.bfloat16)], axis=0)
    slot_shape = (local_experts, sp_size, capacity, model_width)
    x_send = token_pad[source // top_count].reshape(slot_shape)
    c_send = scaled_pad[source].reshape(slot_shape)
    slot_share = capacity // tp_size
    first_slot = lax.axis_index("tp") * slot_share
    x_part = lax.dynamic_slice_in_dim(x_send, first_slot, slot_share, 2)
    c_part = lax.dynamic_slice_in_dim(c_send, first_slot, slot_share, 2)
    x_part, c_part = (
        lax.all_to_all(x_part, "sp", split_axis=1, concat_axis=1, tiled=True),
        lax.all_to_all(c_part, "sp", split_axis=1, concat_axis=1, tiled=True),
    )
    x_recv, c_recv = (
        lax.all_gather(x_part, "tp", axis=2, tiled=True),
        lax.all_gather(c_part, "tp", axis=2, tiled=True),
    )
    grad_gate, grad_up, grad_down, partial_value = expert_grads(
        x_recv.reshape(local_experts, -1, model_width),
        c_recv.reshape(local_experts, -1, model_width),
        w_gate,
        w_up,
        w_down,
    )
    pieces = lax.all_to_all(
        partial_value.reshape(slot_shape), "tp", split_axis=2, concat_axis=0, tiled=True
    )
    summed = jnp.sum(
        pieces.reshape(tp_size, local_experts, sp_size, slot_share, model_width).astype(
            jnp.float32
        ),
        axis=0,
    )
    returned = lax.all_to_all(
        summed.astype(jnp.bfloat16), "sp", split_axis=1, concat_axis=1, tiled=True
    ).astype(summed.dtype)
    offset = position - first_slot
    inside = ((offset >= 0) & (offset < slot_share)).astype(jnp.float32)
    index_part = bucket * slot_share + jnp.clip(offset, 0, slot_share - 1)
    picked = returned.reshape(-1, model_width)[index_part] * inside[:, None]
    token_part = jnp.sum(picked.reshape(tok_rows, top_count, model_width), axis=1)
    routed_total = lax.psum(token_part.astype(jnp.bfloat16), "tp").astype(jnp.float32)
    mid_grad = (out_grad.astype(jnp.float32) + routed_total).astype(jnp.bfloat16)
    gated = (gate_branch.astype(jnp.float32) * states).astype(jnp.bfloat16)
    proj_grad = lax.psum_scatter(
        lax.dot_general(
            mid_grad, gated, (((0,), (0,)), ((), ())), preferred_element_type=jnp.float32
        ).astype(jnp.bfloat16),
        "sp",
        scatter_dimension=0,
        tiled=True,
    ).astype(jnp.float32)
    act_grad = jnp.dot(mid_grad, w_proj, preferred_element_type=jnp.float32)
    branch_grad = (act_grad * states).astype(jnp.bfloat16)
    state_grad = act_grad * gate_branch.astype(jnp.float32)
    channels = decay.shape[1]
    next_decay = jnp.concatenate([decay[1:], jnp.ones((1, channels), jnp.float32)], axis=0)
    decay_prod, local_grad = lax.associative_scan(
        linear_combine, (next_decay[::-1], state_grad[::-1]), axis=0
    )
    decay_prod = decay_prod[::-1]
    local_grad = local_grad[::-1]
    head_decay = decay[0]
    carried = entering(
        (head_decay * decay_prod[0], head_decay * local_grad[0]),
        "sp",
        chain_combine,
        (jnp.ones_like(head_decay), jnp.zeros_like(head_decay)),
    )
    drive_grad = local_grad + decay_prod * carried[1][None, :]
    before = shifted(states[-1:], "sp", 1)
    previous = jnp.concatenate([before, states[:-1]], axis=0)
    decay_grad = drive_grad * previous
    return (grad_gate, grad_up, grad_down, proj_grad, branch_grad, drive_grad, decay_grad)


def solution(mesh):
    placed = (
        P("sp", None),
        P("sp", None),
        P("sp", None),
        P("sp", None),
        P("sp", "tp"),
        P("sp", "tp"),
        P("sp", "tp"),
        P(None, "tp"),
        P("sp", "tp", None),
        P("sp", "tp", None),
        P("sp", "tp", None),
    )
    return jax.shard_map(
        local,
        mesh=mesh,
        in_specs=placed,
        out_specs=(
            P("sp", "tp", None),
            P("sp", "tp", None),
            P("sp", "tp", None),
            P("sp", "tp"),
            P("sp", "tp"),
            P("sp", "tp"),
            P("sp", "tp"),
        ),
        check_vma=False,
    )
```

profile of v0, /device:TPU:0, one launch (start us, length us, event | category | flops | bytes accessed | tf_op | source)
XLA Modules:
  0.0 276.9 jit_solution(13569955936952840303)
XLA Ops:
  13.2 3.3 %gather_fusion.1 = bf16[512,2048]{1,0:T(8,128)(2,1)} fusion(bf16[129,2048]{1,0:T(8,128)(2,1)S(1)} %concatenate.49, s32[1024]{0:T(1024)S(1)} %get-tuple-element.176), kind=kCustom, calls=%fused_computation.1 | custom fusion | bytes 4196352 | tf_op jit(solution)/shard_map/gather | solution.py:105
  17.6 21.7 %all_to_all.27 = bf16[1,8,16,2048]{3,2,0,1:T(8,128)(2,1)} all-to-all(bf16[1,8,16,2048]{3,2,0,1:T(8,128)(2,1)S(1)} %constant_dynamic-slice_fusion.2), channel_id=1, replica_groups=mesh['sp'=8,'tp'=4] {'sp'}, dimensions={1} | all-to-all | bytes 1048576 | tf_op jit(solution)/shard_map/all_to_all | solution.py:112
  39.4 2.4 mul.210
  41.8 3.7 %mul.211 = f32[256,2048]{1,0:T(8,128)} reshape(f32[128,2,2048]{2,1,0:T(2,128)} %mul.210) | data formatting | bytes 4194304 | tf_op jit(solution)/shard_map/mul | solution.py:97
  47.9 3.3 %gather_fusion = bf16[512,2048]{1,0:T(8,128)(2,1)} fusion(bf16[257,2048]{1,0:T(8,128)(2,1)S(1)} %concatenate.48, s32[1024]{0:T(1024)S(1)} %get-tuple-element.177), kind=kCustom, calls=%fused_computation | custom fusion | bytes 4196352 | tf_op jit(solution)/shard_map/gather | solution.py:106
  52.2 17.3 %all_to_all.28 = bf16[1,8,16,2048]{3,2,0,1:T(8,128)(2,1)} all-to-all(bf16[1,8,16,2048]{3,2,0,1:T(8,128)(2,1)S(1)} %constant_dynamic-slice_fusion.3), channel_id=1, replica_groups=mesh['sp'=8,'tp'=4] {'sp'}, dimensions={1} | all-to-all | bytes 1048576 | tf_op jit(solution)/shard_map/all_to_all | solution.py:113
  69.7 3.0 %fusion.5 = f32[512,512]{1,0:T(8,128)S(1)} fusion(bf16[512,2048]{1,0:T(8,128)(2,1)} %bitcast.85, bf16[1,512,2048]{2,1,0:T(8,128)(2,1)S(1)} %copy-done), kind=kOutput, calls=%fused_computation.17 | convolution fusion | flops 1073741824 | bytes 5242880 | tf_op jit(solution)/shard_map/esd,efd->esf/dot_general | solution.py:38
  75.0 16.4 %all-gather.5.cloned.1.call-done = bf16[1,8,64,2048]{3,2,0,1:T(8,128)(2,1)} async-done(((bf16[1,8,16,2048]{3,2,0,1:T(8,128)(2,1)}), bf16[1,8,64,2048]{3,2,0,1:T(8,128)(2,1)}) %all-gather.5.cloned.1.call-update) | async-done | bytes 2097168 | tf_op jit(solution)/shard_map/all_gather | solution.py:117
  91.4 4.0 %multiply_convert_fusion.2 = (bf16[512,512]{1,0:T(8,128)(2,1)S(1)}, bf16[512,512]{1,0:T(8,128)(2,1)S(1)}) fusion(f32[512,512]{1,0:T(8,128)S(1)} %fusion.5, f32[512,512]{1,0:T(8,128)} %fusion.8, bf16[512,2048]{1,0:T(8,128)(2,1)} %bitcast.89, bf16[1,512,2048]{2,1,0:T(8,128)(2,1)} %param.23), kind=kOutput, calls=%fused_computation.28 | convolution fusion | flops 1077149696 | bytes 7340032 | tf_op jit(solution)/shard_map/esd,efd->esf/dot_general | solution.py:43
  98.7 2.5 copy.37
  101.2 3.7 %all-to-all-start.2 = ((bf16[1,8,64,2048]{3,1,0,2:T(8,128)(2,1)}), bf16[1,8,64,2048]{3,1,0,2:T(8,128)(2,1)S(1)}, u32[]{:S(2)}, u32[]{:S(2)}) async-start(bf16[1,8,64,2048]{3,1,0,2:T(8,128)(2,1)} %copy.37), calls=%async_computation.2 | async-start | bytes 4194304 | tf_op jit(solution)/shard_map/all_to_all | solution.py:126
  105.5 3.4 %collective-permute-start = (f32[1,512]{1,0:T(1,128)}, f32[1,512]{1,0:T(1,128)S(1)}, u32[]{:S(2)}, u32[]{:S(2)}) collective-permute-start(f32[1,512]{1,0:T(1,128)} %slice.319), channel_id=1, source_target_pairs={{0,4},{4,8},{8,12},{12,16},{16,20},{20,24},{24,28},{1,5},{5,9},{9,... | collective-permute-start | bytes 6152 | tf_op jit(solution)/shard_map/ppermute | solution.py:26
  108.9 21.7 %all-to-all-done.2 = bf16[1,8,64,2048]{3,1,0,2:T(8,128)(2,1)S(1)} async-done(((bf16[1,8,64,2048]{3,1,0,2:T(8,128)(2,1)}), bf16[1,8,64,2048]{3,1,0,2:T(8,128)(2,1)S(1)}, u32[]{:S(2)}, u32[]{:S(2)}) %all-to-all-start.2) | async-done | bytes 2097184 | tf_op jit(solution)/shard_map/all_to_all | solution.py:126
  132.1 5.6 %all-to-all-start.3 = ((bf16[1,8,16,2048]{3,2,0,1:T(8,128)(2,1)}), bf16[1,8,16,2048]{3,2,0,1:T(8,128)(2,1)S(1)}, u32[]{:S(2)}, u32[]{:S(2)}) async-start(bf16[1,8,16,2048]{3,2,0,1:T(8,128)(2,1)} %copy.38), calls=%async_computation.3 | async-start | bytes 1048576 | tf_op jit(solution)/shard_map/all_to_all | solution.py:135
  141.9 4.3 %fusion = bf16[1,512,2048]{2,1,0:T(8,128)(2,1)} fusion(bf16[512,512]{1,0:T(8,128)(2,1)S(1)} %copy-done.14, bf16[512,2048]{1,0:T(8,128)(2,1)} %bitcast.86), kind=kOutput, calls=%fused_computation.12 | convolution fusion | flops 1074790400 | bytes 4718592 | tf_op jit(solution)/shard_map/esf,esd->efd/dot_general | solution.py:48
  146.3 2.7 fusion.2
  149.0 3.0 %all-to-all-done.3 = bf16[1,8,16,2048]{3,2,0,1:T(8,128)(2,1)S(1)} async-done(((bf16[1,8,16,2048]{3,2,0,1:T(8,128)(2,1)}), bf16[1,8,16,2048]{3,2,0,1:T(8,128)(2,1)S(1)}, u32[]{:S(2)}, u32[]{:S(2)}) %all-to-all-start.3) | async-done | bytes 524320 | tf_op jit(solution)/shard_map/all_to_all | solution.py:135
  155.8 5.6 %multiply_reduce_fusion = bf16[128,2048]{1,0:T(8,128)(2,1)} fusion(f32[128,2,2048]{2,1,0:T(2,128)} %gather.14, f32[128,2]{1,0:T(8,128)S(1)} %copy-done.16), kind=kLoop, calls=%fused_computation.24 | loop fusion | flops 786432 | bytes 2622464 | tf_op jit(solution)/shard_map/reduce_sum | solution.py:142
  161.6 4.2 %fusion.1 = bf16[1,512,2048]{2,1,0:T(8,128)(2,1)} fusion(bf16[512,512]{1,0:T(8,128)(2,1)S(1)} %copy-done.9, bf16[512,2048]{1,0:T(8,128)(2,1)} %bitcast.87), kind=kOutput, calls=%fused_computation.13 | convolution fusion | flops 1074790400 | bytes 4718592 | tf_op jit(solution)/shard_map/esf,esd->efd/dot_general | solution.py:51
  165.8 27.5 %all-reduce.34.cloned.1.call-done = bf16[128,2048]{1,0:T(8,128)(2,1)} async-done(((bf16[128,2048]{1,0:T(8,128)(2,1)}), bf16[128,2048]{1,0:T(8,128)(2,1)}) %all-reduce.34.cloned.1.call-update) | async-done | bytes 524304 | tf_op jit(solution)/shard_map/psum | solution.py:143
  193.3 2.9 %convert_multiply_fusion = (f32[128,512]{1,0:T(8,128)S(1)}, bf16[128,512]{1,0:T(8,128)(2,1)}) fusion(bf16[128,512]{1,0:T(8,128)(2,1)S(1)} %copy-done.10, f32[128,512]{1,0:T(8,128)S(1)} %copy-done.4, bf16[2048,512]{1,0:T(8,128)(2,1)} %param.20, bf16[128,2048]{1,0:T(8,128)(2,1)} %all-reduce.34.cloned.1.call-done, bf16[128,2048]{1,0:T(8,128)(2,1)S(1)} %copy-done.3), kind=kOutput, calls=%fused_computation.33 | convolution fusion | flops 269746176 | bytes 3932160 | tf_op jit(solution)/shard_map/dot_general | solution.py:154
  202.2 26.2 %all-gather = f32[8,1,512]{2,1,0:T(1,128)S(1)} all-gather(f32[1,1,512]{2,1,0:T(1,128)S(1)} %get-tuple-element.137), channel_id=1, replica_groups=mesh['sp'=8,'tp'=4] {'sp'}, dimensions={0}, use_global_device_ids=true | all-gather | bytes 18432 | tf_op jit(solution)/shard_map/all_gather | solution.py:9
  228.5 26.1 %all-gather.1 = f32[8,1,512]{2,1,0:T(1,128)S(1)} all-gather(f32[1,1,512]{2,1,0:T(1,128)S(1)} %get-tuple-element.136), channel_id=1, replica_groups=mesh['sp'=8,'tp'=4] {'sp'}, dimensions={0}, use_global_device_ids=true | all-gather | bytes 18432 | tf_op jit(solution)/shard_map/all_gather | solution.py:9
  260.9 7.6 %reduce-scatter.2.cloned.1.call-done = bf16[256,512]{1,0:T(8,128)(2,1)} async-done(((bf16[2048,512]{1,0:T(8,128)(2,1)}), bf16[256,512]{1,0:T(8,128)(2,1)}) %reduce-scatter.2.cloned.1.call-update) | async-done | bytes 262160 | tf_op jit(solution)/shard_map/reduce_scatter | solution.py:146
  (235 shorter events, 39.9 us)
Async XLA Ops:
  7.2 62.5 %copy-start = (bf16[1,512,2048]{2,1,0:T(8,128)(2,1)S(1)}, bf16[1,512,2048]{2,1,0:T(8,128)(2,1)}, u32[]{:S(2)}) copy-start(bf16[1,512,2048]{2,1,0:T(8,128)(2,1)} %param.21) | copy-start | bytes 6291460
  7.2 62.4 %all-gather.7.cloned.1.call-start = ((), (), s32[]{:S(2)}) async-start(), calls=%async_computation.6 | async-start | bytes 2621440 | tf_op jit(solution)/shard_map/all_gather | solution.py:116
  16.4 22.9 %copy-start.2 = (bf16[128,2048]{1,0:T(8,128)(2,1)S(1)}, bf16[128,2048]{1,0:T(8,128)(2,1)}, u32[]{:S(2)}) copy-start(bf16[128,2048]{1,0:T(8,128)(2,1)} %param.14) | copy-start | bytes 1572868
  39.3 52.1 %all-gather.5.cloned.1.call-start = ((), (), s32[]{:S(2)}) async-start(), calls=%async_computation.5 | async-start | bytes 2621440 | tf_op jit(solution)/shard_map/all_gather | solution.py:117
  41.7 3.7 %copy-start.17 = (f32[128,2]{0,1:T(2,128)S(1)}, f32[128,2]{0,1:T(2,128)}, u32[]{:S(2)}) copy-start(f32[128,2]{0,1:T(2,128)} %param.16) | copy-start | bytes 3076
  69.6 3.1 %copy-start.6 = (bf16[1,512,2048]{2,1,0:T(8,128)(2,1)S(1)}, bf16[1,512,2048]{2,1,0:T(8,128)(2,1)}, u32[]{:S(2)}) copy-start(bf16[1,512,2048]{2,1,0:T(8,128)(2,1)} %param.22) | copy-start | bytes 6291460
  69.6 3.0 %copy-start.18 = (bf16[1,8,64,2048]{3,2,0,1:T(8,128)(2,1)S(1)}, bf16[1,8,64,2048]{3,2,0,1:T(8,128)(2,1)}, u32[]{:S(2)}) copy-start(bf16[1,8,64,2048]{3,2,0,1:T(8,128)(2,1)} %all-gather.7.cloned.1.call-done) | copy-start | bytes 6291460
  72.7 18.7 %copy-start.20 = (f32[512,512]{1,0:T(8,128)}, f32[512,512]{1,0:T(8,128)S(1)}, u32[]{:S(2)}) copy-start(f32[512,512]{1,0:T(8,128)S(1)} %fusion.5) | copy-start | bytes 3145732
  101.2 3.8 %copy-start.4 = (f32[128,512]{1,0:T(8,128)S(1)}, f32[128,512]{1,0:T(8,128)}, u32[]{:S(2)}) copy-start(f32[128,512]{1,0:T(8,128)} %param.18) | copy-start | bytes 786436
  101.2 29.4 %all-to-all-start.2 = ((bf16[1,8,64,2048]{3,1,0,2:T(8,128)(2,1)}), bf16[1,8,64,2048]{3,1,0,2:T(8,128)(2,1)S(1)}, u32[]{:S(2)}, u32[]{:S(2)}) async-start(bf16[1,8,64,2048]{3,1,0,2:T(8,128)(2,1)} %copy.37), calls=%async_computation.2 | async-start | bytes 4194304 | tf_op jit(solution)/shard_map/all_to_all | solution.py:126
  105.5 154.5 %collective-permute-start = (f32[1,512]{1,0:T(1,128)}, f32[1,512]{1,0:T(1,128)S(1)}, u32[]{:S(2)}, u32[]{:S(2)}) collective-permute-start(f32[1,512]{1,0:T(1,128)} %slice.319), channel_id=1, source_target_pairs={{0,4},{4,8},{8,12},{12,16},{16,20},{20,24},{24,28},{1,5},{5,9},{9,... | collective-permute-start | bytes 6152 | tf_op jit(solution)/shard_map/ppermute | solution.py:26
  130.6 7.5 %copy-start.15 = (f32[128,512]{1,0:T(8,128)S(1)}, f32[128,512]{1,0:T(8,128)}, u32[]{:S(2)}) copy-start(f32[128,512]{1,0:T(8,128)} %param.19) | copy-start | bytes 786436
  132.1 9.8 %copy-start.14 = (bf16[512,512]{1,0:T(8,128)(2,1)S(1)}, bf16[512,512]{1,0:T(8,128)(2,1)}, u32[]{:S(2)}) copy-start(bf16[512,512]{1,0:T(8,128)(2,1)} %copy-done.13) | copy-start | bytes 1572868
  132.1 19.9 %all-to-all-start.3 = ((bf16[1,8,16,2048]{3,2,0,1:T(8,128)(2,1)}), bf16[1,8,16,2048]{3,2,0,1:T(8,128)(2,1)S(1)}, u32[]{:S(2)}, u32[]{:S(2)}) async-start(bf16[1,8,16,2048]{3,2,0,1:T(8,128)(2,1)} %copy.38), calls=%async_computation.3 | async-start | bytes 1048576 | tf_op jit(solution)/shard_map/all_to_all | solution.py:135
  137.7 55.6 %all-reduce.34.cloned.1.call-start = ((), (), s32[]{:S(2)}) async-start(), calls=%async_computation.7 | async-start | bytes 1048576 | tf_op jit(solution)/shard_map/psum | solution.py:143
  141.9 4.4 %copy-start.19 = (bf16[1,8,64,2048]{3,2,0,1:T(8,128)(2,1)S(1)}, bf16[1,8,64,2048]{3,2,0,1:T(8,128)(2,1)}, u32[]{:S(2)}) copy-start(bf16[1,8,64,2048]{3,2,0,1:T(8,128)(2,1)} %all-gather.5.cloned.1.call-done) | copy-start | bytes 6291460
  141.9 4.4 %copy-start.21 = (f32[512,512]{1,0:T(8,128)S(1)}, f32[512,512]{1,0:T(8,128)}, u32[]{:S(2)}) copy-start(f32[512,512]{1,0:T(8,128)} %copy-done.20) | copy-start | bytes 3145732
  141.9 4.4 %copy-start.22 = (f32[512,512]{1,0:T(8,128)S(1)}, f32[512,512]{1,0:T(8,128)}, u32[]{:S(2)}) copy-start(f32[512,512]{1,0:T(8,128)} %fusion.8) | copy-start | bytes 3145732
  155.8 5.7 %copy-start.9 = (bf16[512,512]{1,0:T(8,128)(2,1)S(1)}, bf16[512,512]{1,0:T(8,128)(2,1)}, u32[]{:S(2)}) copy-start(bf16[512,512]{1,0:T(8,128)(2,1)} %copy-done.8) | copy-start | bytes 1572868
  161.5 31.8 %copy-start.3 = (bf16[128,2048]{1,0:T(8,128)(2,1)S(1)}, bf16[128,2048]{1,0:T(8,128)(2,1)}, u32[]{:S(2)}) copy-start(bf16[128,2048]{1,0:T(8,128)(2,1)} %param.14) | copy-start | bytes 1572868
  161.5 31.8 %copy-start.10 = (bf16[128,512]{1,0:T(8,128)(2,1)S(1)}, bf16[128,512]{1,0:T(8,128)(2,1)}, u32[]{:S(2)}) copy-start(bf16[128,512]{1,0:T(8,128)(2,1)} %param.17) | copy-start | bytes 393220
  161.5 107.0 %reduce-scatter.2.cloned.1.call-start = ((), (), s32[]{:S(2)}) async-start(), calls=%async_computation.8 | async-start | bytes 2359296 | tf_op jit(solution)/shard_map/reduce_scatter | solution.py:146
  165.8 30.9 %copy-start.11 = (f32[64,512]{1,0:T(8,128)S(1)}, f32[64,512]{1,0:T(8,128)}, u32[]{:S(2)}) copy-start(f32[64,512]{1,0:T(8,128)} %slice.251) | copy-start | bytes 393220
  255.1 15.2 %copy-start.1 = (bf16[1,512,2048]{2,1,0:T(8,128)(2,1)S(1)}, bf16[1,512,2048]{2,1,0:T(8,128)(2,1)}, u32[]{:S(2)}) copy-start(bf16[1,512,2048]{2,1,0:T(8,128)(2,1)} %param.21) | copy-start | bytes 6291460
  (6 other events, 9.1 us)
Sparse Core Ops, SparseCore 0:
  39.4 21.5 all-gather.6
  69.7 21.6 all-gather.4
  161.6 31.6 all-reduce.33
  199.7 68.7 reduce-scatter.1
where the time goes:
time: 278 us; the launch traced here: 277 us
  blocking collectives  91.4 us (33%)
  waiting for transfers between devices  76.3 us (27%)
  local copies, waits for them, and re-layouts  37.5 us (13%)
  matrix products  28.1 us (10%)
  other arithmetic  15.3 us (6%)
  between operations  14.8 us (5%)
  starting transfers between devices  13.1 us (5%)
    all_gather x2, blocking collectives, entering(): pieces = jax.tree.map(lambda part: lax.all_gather(part, axis), value)  52.4 us
    psum x1, waiting for transfers between devices, local(): lax.psum(token_part.astype(jnp.bfloat16), 'tp').astype(jnp.float32)  27.5 us
    all_to_all x1, blocking collectives, local(): lax.all_to_all(x_part, 'sp', split_axis=1, concat_axis=1, tiled=True)  21.7 us
    all_to_all x1, waiting for transfers between devices, local(): lax.all_to_all(partial_value.reshape(slot_shape), 'tp', split_axis=2, con...  21.7 us
    all_to_all x1, blocking collectives, local(): lax.all_to_all(c_part, 'sp', split_axis=1, concat_axis=1, tiled=True)  17.3 us
    all_gather x1, waiting for transfers between devices, local(): lax.all_gather(c_part, 'tp', axis=2, tiled=True)  16.4 us
    reduce_scatter x1, waiting for transfers between devices, local(): lax.psum_scatter(lax.dot_general(mid_grad, gated, (((0,), (0,)), ((), ())...  7.59 us
    mul x3, local copies, waits for them, and re-layouts, local(): route_weights[:, :, None] * out_grad[:, None, :].astype(jnp.float32)  6.17 us
  transfers between devices with their start and end apart: 7, of which 5 were waited for; matrix products, arithmetic and copies ran while one was open for 21% of the time, Pallas kernels for 0%

commit v1 on v0

v1 whole, which is shorter than its diff:
```python
import functools

import jax
import jax.numpy as jnp
from jax import lax
from jax.experimental import pallas as pl
from jax.experimental.pallas import tpu as pltpu
from jax.sharding import PartitionSpec as P

MESH = pl.DeviceIdType.MESH
F32 = jnp.float32
BF16 = jnp.bfloat16
CHUNKS = 2


def dot(a, b, ca, cb):
    return lax.dot_general(a, b, (((ca,), (cb,)), ((), ())), preferred_element_type=F32)


def kernel(
    n_sp,
    n_tp,
    ids,
    wts,
    mix,
    og,
    gb,
    st,
    dc,
    wp_h,
    wg_h,
    wu_h,
    wd_h,
    dwg_h,
    dwu_h,
    dwd_h,
    gproj,
    gbr,
    gdr,
    gdc,
    wp,
    wg,
    wu,
    wd,
    dwg,
    dwu,
    dwd,
    sel,
    send,
    xc,
    ga,
    pv,
    gg,
    ug,
    hid,
    pb,
    po,
    rc,
    qb,
    ry,
    fb,
    ret,
    mt,
    mr,
    cs,
    cr,
    w_sem,
    o_sem,
    l_sem,
    sp_s,
    sp_r,
    core_s,
    core_r,
    y_s,
    y_r,
    ga_s,
    ga_r,
    pv_sem,
    pc_s,
    pc_r,
    py_s,
    py_r,
    ret_s,
    ret_r,
    mt_s,
    mt_r,
    mr_s,
    mr_r,
    c_s,
    c_r,
):
    i = lax.axis_index("sp")
    t = lax.axis_index("tp")
    ny = n_tp // 2
    y, c = t // 2, t % 2
    tok = mix.shape[0]
    cap = xc.shape[3]
    dg = xc.shape[4]
    half = n_sp // CHUNKS
    rows = half * cap
    slots = n_sp * cap
    peer = (i, y * 2 + 1 - c)

    def columns(g):
        return pl.ds(pl.multiple_of(g * dg, dg), dg)

    def later(k):
        return lax.rem(i + k, n_sp)

    def before(k):
        return lax.rem(i + n_sp - k, n_sp)

    def y_up(q):
        return lax.rem(y + q, ny)

    def remote(src, dst, s, r, who):
        return pltpu.make_async_remote_copy(
            src_ref=src, dst_ref=dst, send_sem=s, recv_sem=r, device_id=who, device_id_type=MESH
        )

    loads = [
        pltpu.make_async_copy(a, b, w_sem.at[n])
        for n, (a, b) in enumerate(((wg_h, wg), (wu_h, wu), (wd_h, wd), (wp_h, wp)))
    ]
    for load in loads:
        load.start()

    barrier = pltpu.get_barrier_semaphore()
    for k in range(1, n_sp):
        pl.semaphore_signal(barrier, inc=1, device_id=(later(k), t), device_id_type=MESH)
    for k in range(1, n_tp):
        pl.semaphore_signal(
            barrier, inc=1, device_id=(i, lax.rem(t + k, n_tp)), device_id_type=MESH
        )

    experts_iota = lax.broadcasted_iota(jnp.int32, (n_sp, tok), 0)
    named = jnp.zeros((n_sp, tok), F32)
    weight = jnp.zeros((n_sp, tok), F32)
    for k in range(ids.shape[0]):
        hit = ids[k : k + 1, :] == experts_iota
        named = jnp.where(hit, 1.0, named)
        weight = jnp.where(hit, wts[k : k + 1, :], weight)
    earlier = (
        lax.broadcasted_iota(jnp.int32, (tok, tok), 0)
        < lax.broadcasted_iota(jnp.int32, (tok, tok), 1)
    )
    place = dot(named.astype(BF16), jnp.where(earlier, 1.0, 0.0).astype(BF16), 1, 0)
    place = jnp.where(named > 0.5, place, -1.0).astype(jnp.int32)
    slot_iota = lax.broadcasted_iota(jnp.int32, (cap, tok), 0)
    mix_part = mix[:, columns(t)]
    og_part = og[:, columns(t)]
    for e in range(n_sp):
        here = jnp.where(place[e : e + 1, :] == slot_iota, 1.0, 0.0)
        slot_weight = jnp.sum(here * weight[e : e + 1, :], axis=1, keepdims=True)
        here = here.astype(BF16)
        sel[e * cap : (e + 1) * cap, :] = here
        send[0, e] = dot(here, mix_part, 1, 0).astype(BF16)
        send[1, e] = (dot(here, og_part, 1, 0) * slot_weight).astype(BF16)

    ga[i] = (gb[...].astype(F32) * st[...]).astype(BF16)
    pl.semaphore_wait(barrier, n_sp + n_tp - 2)

    pending = []

    def go(copy):
        copy.start()
        pending.append(copy)

    own = pltpu.make_async_copy(send.at[:, i], xc.at[:, t, i], l_sem.at[0])
    own.start()

    def dispatch(k):
        return remote(
            send.at[:, later(k)], xc.at[:, t, i], sp_s.at[k], sp_r.at[k], (later(k), t)
        )

    for k in range(1, n_sp):
        go(dispatch(k))
    go(
        remote(
            st.at[pl.ds(tok - 8, 8)], pv, pv_sem.at[0], pv_sem.at[1], (later(1), t)
        )
    )
    pv_copy = pending[-1]

    def to_core(q, k):
        block = xc.at[:, 2 * y_up(q) + c, before(k)]
        return remote(block, block, core_s.at[q, k], core_r.at[q, k], peer)

    def to_y(q, k):
        block = xc.at[:, t, before(k)]
        return remote(
            block, block, y_s.at[q, k], y_r.at[q, k], (i, 2 * y_up(q) + c)
        )

    def from_y(q, k):
        block = xc.at[:, 2 * y_up(ny - q) + c, before(k)]
        return remote(block, block, y_s.at[q, k], y_r.at[q, k], (i, 2 * y_up(q) + c))

    def from_sp(k):
        return remote(
            send.at[:, later(k)], xc.at[:, t, before(k)], sp_s.at[k], sp_r.at[k], (later(k), t)
        )

    def from_core(q, k):
        block = xc.at[:, 2 * y_up(q) + 1 - c, before(k)]
        return remote(block, block, core_s.at[q, k], core_r.at[q, k], peer)

    def spread(k):
        if k == 0:
            own.wait()
        else:
            from_sp(k).wait_recv()
        for q in range(1, ny):
            go(to_y(q, k))
        go(to_core(0, k))

    def hand_on(k):
        for q in range(1, ny):
            from_y(q, k).wait_recv()
            go(to_core(ny - q, k))

    def expert(m):
        order = [before(m * half + q) for q in range(half)]

        def rows_of(which, g):
            return jnp.concatenate([xc[which, g, s] for s in order], axis=0)

        gate = up = hg = None
        for g in range(n_tp):
            cols = slice(g * dg, (g + 1) * dg)
            x, cot = rows_of(0, g), rows_of(1, g)
            parts = (dot(x, wg[:, cols], 1, 1), dot(x, wu[:, cols], 1, 1), dot(cot, wd[:, cols], 1, 1))
            if g == 0:
                gate, up, hg = parts
            else:
                gate, up, hg = gate + parts[0], up + parts[1], hg + parts[2]
        s = jax.nn.sigmoid(gate)
        silu = gate * s
        hidden = (silu * up).astype(BF16)
        up_grad = (hg * silu).astype(BF16)
        gate_grad = (hg * up * s * (1.0 + gate * (1.0 - s))).astype(BF16)
        for q, src in enumerate(order):
            part = slice(q * cap, (q + 1) * cap)
            hid[src] = hidden[part]
            ug[src] = up_grad[part]
            gg[src] = gate_grad[part]
        return gate_grad, up_grad

    def partial(gate_grad, up_grad, g):
        cols = columns(g)
        return (dot(gate_grad, wg[:, cols], 1, 0) + dot(up_grad, wu[:, cols], 1, 0)).astype(BF16)

    def swap_core(m, q):
        return remote(pb.at[m, q], rc.at[m, q], pc_s.at[m, q], pc_r.at[m, q], peer)

    def swap_y(m, q):
        return remote(
            qb.at[m, q], ry.at[m, q], py_s.at[m, q], py_r.at[m, q], (i, 2 * y_up(q) + c)
        )

    def partials(m, grads):
        for q in list(range(1, ny)) + [0]:
            pb[m, q] = partial(*grads, 2 * y_up(q) + 1 - c)
            go(swap_core(m, q))
        for q in list(range(1, ny)) + [0]:
            po[m, q] = partial(*grads, 2 * y_up(q) + c)

    def fold_core(m):
        for q in range(1, ny):
            swap_core(m, q).wait_recv()
            qb[m, q] = (po[m, q].astype(F32) + rc[m, q].astype(F32)).astype(BF16)
            go(swap_y(m, q))

    def home(k):
        m, q = k // half, k % half
        return remote(
            fb.at[m, pl.ds(q * cap, cap)], ret.at[i], ret_s.at[k], ret_r.at[k], (before(k), t)
        )

    def fold_y(m):
        swap_core(m, 0).wait_recv()
        total = po[m, 0].astype(F32) + rc[m, 0].astype(F32)
        for q in range(1, ny):
            swap_y(m, q).wait_recv()
            total = total + ry[m, q].astype(F32)
        fb[m] = total.astype(BF16)
        for q in range(half):
            k = m * half + q
            if k == 0:
                pltpu.make_async_copy(
                    fb.at[0, pl.ds(0, cap)], ret.at[i], l_sem.at[1]
                ).start()
            else:
                go(home(k))

    def weight_grad(left, which, out, out_h, n):
        a = left[...].reshape(slots, left.shape[2])
        for g in range(n_tp):
            b = xc[which, g].reshape(slots, dg)
            out[:, g * dg : (g + 1) * dg] = dot(a, b, 0, 0).astype(BF16)
        copy = pltpu.make_async_copy(out, out_h, o_sem.at[n])
        copy.start()
        return copy

    for k in range(n_sp):
        spread(k)
        if k >= 1:
            hand_on(k - 1)
    hand_on(n_sp - 1)

    def share_gated(k):
        return remote(ga.at[i], ga.at[i], ga_s.at[k], ga_r.at[k], (later(k), t))

    for k in range(1, n_sp):
        go(share_gated(k))
    for load in loads:
        load.wait()

    def arrived(m):
        for k in range(m * half, (m + 1) * half):
            for q in range(ny):
                from_core(q, k).wait_recv()

    arrived(0)
    grads = expert(0)
    partials(0, grads)
    arrived(1)
    grads = expert(1)
    fold_core(0)
    partials(1, grads)
    outs = [weight_grad(gg, 0, dwg, dwg_h, 0)]
    fold_core(1)
    fold_y(0)
    outs.append(weight_grad(ug, 0, dwu, dwu_h, 1))
    fold_y(1)
    outs.append(weight_grad(hid, 1, dwd, dwd_h, 2))

    pltpu.make_async_copy(fb.at[0, pl.ds(0, cap)], ret.at[i], l_sem.at[1]).wait()

    def from_expert(k):
        m, q = k // half, k % half
        return remote(
            fb.at[m, pl.ds(q * cap, cap)],
            ret.at[later(k)],
            ret_s.at[k],
            ret_r.at[k],
            (before(k), t),
        )

    for k in range(1, n_sp):
        from_expert(k).wait_recv()
    routed = dot(ret[...].reshape(slots, dg), sel[...], 0, 0)
    mid = (og[:, columns(t)].astype(F32).T + routed).astype(BF16)
    mt[t] = mid

    def share_mid(k):
        return remote(mt.at[t], mt.at[t], mt_s.at[k], mt_r.at[k], (i, lax.rem(t + k, n_tp)))

    def get_mid(k):
        block = mt.at[lax.rem(t + n_tp - k, n_tp)]
        return remote(block, block, mt_s.at[k], mt_r.at[k], (i, lax.rem(t + k, n_tp)))

    for k in range(1, n_tp):
        go(share_mid(k))

    row = lax.broadcasted_iota(jnp.int32, dc.shape, 0)
    decay = dc[...]
    head = decay[0:1, :]
    factor = jnp.where(row < tok - 1, pltpu.roll(decay, tok - 1, 0), 1.0)
    for k in range(1, n_tp):
        get_mid(k).wait_recv()

    share = mr.shape[1]
    per = dg // share if dg >= share else 1

    def rows_for(s):
        return mt.at[s // per, pl.ds(pl.multiple_of((s % per) * share, share), share)]

    def share_rows(k):
        return remote(rows_for(later(k)), mr.at[i], mr_s.at[k], mr_r.at[k], (later(k), t))

    def get_rows(k):
        return remote(rows_for(later(k)), mr.at[before(k)], mr_s.at[k], mr_r.at[k], (later(k), t))

    for k in range(1, n_sp):
        go(share_rows(k))
    own_rows = pltpu.make_async_copy(rows_for(i), mr.at[i], l_sem.at[2])
    own_rows.start()

    act = dot(mt[...].reshape(n_tp * dg, tok), wp[...], 0, 0)
    grad = act * gb[...].astype(F32)
    gbr[...] = (act * st[...]).astype(BF16)
    step = 1
    while step < tok:
        inside = row < tok - step
        grad = grad + jnp.where(inside, factor * pltpu.roll(grad, tok - step, 0), 0.0)
        factor = factor * jnp.where(inside, pltpu.roll(factor, tok - step, 0), 1.0)
        step *= 2
    pair = jnp.concatenate([head * factor[0:1, :], head * grad[0:1, :]], axis=0)
    pair = jnp.concatenate([pair, jnp.zeros((6, pair.shape[1]), F32)], axis=0)
    cs[...] = pair
    cr[i] = pair

    def share_carry(k):
        return remote(cs, cr.at[i], c_s.at[k], c_r.at[k], (later(k), t))

    def get_carry(k):
        return remote(cs, cr.at[before(k)], c_s.at[k], c_r.at[k], (later(k), t))

    for k in range(1, n_sp):
        go(share_carry(k))

    own_rows.wait()
    for k in range(1, n_sp):
        remote(ga.at[i], ga.at[before(k)], ga_s.at[k], ga_r.at[k], (later(k), t)).wait_recv()
    total = None
    for k in range(n_sp):
        if k:
            get_rows(k).wait_recv()
        src = before(k)
        term = dot(mr[src], ga[src], 1, 0)
        total = term if total is None else total + term
    gproj[...] = total

    for k in range(1, n_sp):
        get_carry(k).wait_recv()
    carry = jnp.zeros((1, pair.shape[1]), F32)
    for s in range(n_sp - 1, 0, -1):
        carry = jnp.where(s > i, cr[s, 1:2, :] + cr[s, 0:1, :] * carry, carry)
    drive = grad + factor * carry
    gdr[...] = drive
    pv_copy.wait_recv()
    states = st[...]
    last = jnp.where(i > 0, pv[7:8, :], 0.0)
    previous = jnp.where(row == 0, last, pltpu.roll(states, 1, 0))
    gdc[...] = drive * previous

    for copy in outs:
        copy.wait()
    for copy in pending:
        copy.wait_send()


def local(
    mixer_out,
    out_grad,
    route_ids,
    route_weights,
    gate_branch,
    states,
    decay,
    w_proj,
    w_gate,
    w_up,
    w_down,
):
    tok, width = mixer_out.shape
    top = route_ids.shape[1]
    n_sp, n_tp = lax.axis_size("sp"), lax.axis_size("tp")
    ny = n_tp // 2
    assert w_gate.shape[0] == 1
    cap = 2 * top * tok // n_sp
    dg = width // n_tp
    hidden = w_gate.shape[1]
    channels = states.shape[1]
    half_rows = n_sp * cap // CHUNKS
    share = width // n_sp
    vmem = pl.BlockSpec(memory_space=pltpu.VMEM)
    hbm = pl.BlockSpec(memory_space=pl.ANY)
    dma = pltpu.SemaphoreType.DMA
    weight = (hidden, width)
    outs = pl.pallas_call(
        functools.partial(kernel, n_sp, n_tp),
        out_shape=[jax.ShapeDtypeStruct(weight, BF16)] * 3
        + [
            jax.ShapeDtypeStruct((share, channels), F32),
            jax.ShapeDtypeStruct((tok, channels), BF16),
            jax.ShapeDtypeStruct((tok, channels), F32),
            jax.ShapeDtypeStruct((tok, channels), F32),
        ],
        in_specs=[vmem] * 7 + [hbm] * 4,
        out_specs=[hbm] * 3 + [vmem] * 4,
        scratch_shapes=[
            pltpu.VMEM((width, channels), BF16),
            *([pltpu.VMEM(weight, BF16)] * 6),
            pltpu.VMEM((n_sp * cap, tok), BF16),
            pltpu.VMEM((2, n_sp, cap, dg), BF16),
            pltpu.VMEM((2, n_tp, n_sp, cap, dg), BF16),
            pltpu.VMEM((n_sp, tok, channels), BF16),
            pltpu.VMEM((8, channels), F32),
            *([pltpu.VMEM((n_sp, cap, hidden), BF16)] * 3),
            *([pltpu.VMEM((CHUNKS, ny, half_rows, dg), BF16)] * 5),
            pltpu.VMEM((CHUNKS, half_rows, dg), BF16),
            pltpu.VMEM((n_sp, cap, dg), BF16),
            pltpu.VMEM((n_tp, dg, tok), BF16),
            pltpu.VMEM((n_sp, share, tok), BF16),
            pltpu.VMEM((8, channels), F32),
            pltpu.VMEM((n_sp, 8, channels), F32),
            dma((4,)),
            dma((3,)),
            dma((3,)),
            dma((n_sp,)),
            dma((n_sp,)),
            *([dma((ny, n_sp))] * 4),
            dma((n_sp,)),
            dma((n_sp,)),
            dma((2,)),
            *([dma((CHUNKS, ny))] * 4),
            dma((n_sp,)),
            dma((n_sp,)),
            dma((n_tp,)),
            dma((n_tp,)),
            *([dma((n_sp,))] * 4),
        ],
        compiler_params=pltpu.CompilerParams(
            collective_id=0, has_side_effects=True, vmem_limit_bytes=60 * 1024 * 1024
        ),
    )(
        route_ids.T,
        route_weights.T,
        mixer_out,
        out_grad,
        gate_branch,
        states,
        decay,
        w_proj,
        w_gate[0],
        w_up[0],
        w_down[0],
    )
    return (outs[0][None], outs[1][None], outs[2][None], *outs[3:])


def solution(mesh):
    placed = (
        P("sp", None),
        P("sp", None),
        P("sp", None),
        P("sp", None),
        P("sp", "tp"),
        P("sp", "tp"),
        P("sp", "tp"),
        P(None, "tp"),
        P("sp", "tp", None),
        P("sp", "tp", None),
        P("sp", "tp", None),
    )
    return jax.shard_map(
        local,
        mesh=mesh,
        in_specs=placed,
        out_specs=(
            P("sp", "tp", None),
            P("sp", "tp", None),
            P("sp", "tp", None),
            P("sp", "tp"),
            P("sp", "tp"),
            P("sp", "tp"),
            P("sp", "tp"),
        ),
        check_vma=False,
    )
```

time: 278 us -> 106 us (0.38)
  Pallas kernels: 0 us -> 95.6 us
  blocking collectives: 91.4 us -> 0 us
  waiting for transfers between devices: 76.3 us -> 0 us
  matrix products: 28.1 us -> 0 us
  local copies, waits for them, and re-layouts: 37.5 us -> 9.86 us
  other arithmetic: 15.3 us -> 0 us
  between operations: 14.8 us -> 0.66 us
  starting transfers between devices: 13.1 us -> 0 us
    pallas_call x0 -> x1, Pallas kernels: none -> 95.6 us  [local(): pl.pallas_call(functools.partial(kernel, n_sp, n_tp), out_shape=[jax.Shap...]
    all_gather x2 -> x0, blocking collectives: 52.4 us -> none  [entering(): pieces = jax.tree.map(lambda part: lax.all_gather(part, axis), value)]
    all_to_all x2 -> x0, blocking collectives: 39 us -> none  [the longest x1 21.7 us: local(): lax.all_to_all(x_part, 'sp', split_axis=1, concat_axis=1, tiled=True)]
    dot_general x10 -> x0, matrix products: 28.1 us -> none  [the longest x1 4.34 us: expert_grads(): jnp.einsum('esf,esd->efd', gate_grad, inputs, preferred_element_type=jnp....]
    psum x1 -> x0, waiting for transfers between devices: 27.5 us -> none  [local(): lax.psum(token_part.astype(jnp.bfloat16), 'tp').astype(jnp.float32)]
    all_to_all x2 -> x0, waiting for transfers between devices: 24.7 us -> none  [the longest x1 21.7 us: local(): lax.all_to_all(partial_value.reshape(slot_shape), 'tp', split_axis=2, con...]
    all_gather x2 -> x0, waiting for transfers between devices: 16.5 us -> none  [the longest x1 16.4 us: local(): lax.all_gather(c_part, 'tp', axis=2, tiled=True)]
    gather x4 -> x0, local copies, waits for them, and re-layouts: 10.3 us -> none  [the longest x2 3.69 us: local(): picked = returned.reshape(-1, model_width)[index_part] * inside[:, None]]
  transfers between devices with their start and end apart: 7 -> 0, of which waited for: 5 -> 0; matrix products, arithmetic and copies ran while one was open for 21% -> 0% of each run, Pallas kernels for 0% -> 0%
where the time goes in v1:
time: 106 us
  Pallas kernels  95.6 us (90%)
  local copies, waits for them, and re-layouts  9.86 us (9%)
    pallas_call x1, Pallas kernels, local(): pl.pallas_call(functools.partial(kernel, n_sp, n_tp), out_shape=[jax.Shap...  95.6 us
    unnamed x19, local copies, waits for them, and re-layouts  9.86 us

profile of v1, /device:TPU:0, one launch (start us, length us, event | category | flops | bytes accessed | tf_op | source)
XLA Modules:
  0.0 106.1 jit_solution(197662237432327611)
XLA Ops:
  0.6 95.6 %shard_map.162 = (bf16[512,2048]{1,0:T(8,128)(2,1)}, bf16[512,2048]{1,0:T(8,128)(2,1)}, bf16[512,2048]{1,0:T(8,128)(2,1)}, f32[256,512]{1,0:T(8,128)}, bf16[128,...) custom-call(s32[2,128]{1,0:T(2,128)} %bitcast.14, f32[2,128]{1,0:T(2,128)} %bitcast.15, ...), custom_call_target="tpu_custom_call" | custom-call | tf_op jit(solution)/shard_map/pallas_call | solution.py:473
  96.2 0.0 copy-start.1
  96.2 3.3 %copy.25 = bf16[1,512,2048]{2,1,0:T(8,128)(2,1)} copy(bf16[1,512,2048]{2,1,0:T(8,128)(2,1)} %bitcast.10) | data formatting | bytes 4194304
  99.5 0.0 copy-done.1
  99.5 0.0 copy-start
  99.5 1.3 %copy.26 = bf16[1,512,2048]{2,1,0:T(8,128)(2,1)} copy(bf16[1,512,2048]{2,1,0:T(8,128)(2,1)S(1)} %bitcast.9) | data formatting | bytes 4194304
  100.9 1.0 copy-done
  101.9 0.0 copy-start.2
  101.9 0.0 copy-start.5
  101.9 0.0 copy-start.4
  101.9 0.0 copy-start.3
  101.9 1.3 %copy.27 = bf16[1,512,2048]{2,1,0:T(8,128)(2,1)} copy(bf16[1,512,2048]{2,1,0:T(8,128)(2,1)S(1)} %bitcast.8) | data formatting | bytes 4194304
  103.2 0.0 copy-done.2
  103.2 0.8 copy.28
  104.0 0.0 copy-done.5
  104.0 0.7 copy.29
  104.7 0.0 copy-done.4
  104.7 0.7 copy.30
  105.4 0.0 copy-done.3
  105.4 0.7 copy.31
Async XLA Ops:
  96.2 3.3 %copy-start.1 = (bf16[512,2048]{1,0:T(8,128)(2,1)S(1)}, bf16[512,2048]{1,0:T(8,128)(2,1)}, u32[]{:S(2)}) copy-start(bf16[512,2048]{1,0:T(8,128)(2,1)} %get-tuple-element.15) | copy-start | bytes 6291460
  99.5 2.3 %copy-start = (bf16[512,2048]{1,0:T(8,128)(2,1)S(1)}, bf16[512,2048]{1,0:T(8,128)(2,1)}, u32[]{:S(2)}) copy-start(bf16[512,2048]{1,0:T(8,128)(2,1)} %get-tuple-element.16) | copy-start | bytes 6291460
  101.9 1.3 %copy-start.2 = (f32[256,512]{1,0:T(8,128)S(1)}, f32[256,512]{1,0:T(8,128)}, u32[]{:S(2)}) copy-start(f32[256,512]{1,0:T(8,128)} %get-tuple-element.31) | copy-start | bytes 1572868
  101.9 2.1 %copy-start.5 = (bf16[128,512]{1,0:T(8,128)(2,1)S(1)}, bf16[128,512]{1,0:T(8,128)(2,1)}, u32[]{:S(2)}) copy-start(bf16[128,512]{1,0:T(8,128)(2,1)} %get-tuple-element.32) | copy-start | bytes 393220
  101.9 2.8 %copy-start.4 = (f32[128,512]{1,0:T(8,128)S(1)}, f32[128,512]{1,0:T(8,128)}, u32[]{:S(2)}) copy-start(f32[128,512]{1,0:T(8,128)} %get-tuple-element.33) | copy-start | bytes 786436
  101.9 3.5 %copy-start.3 = (f32[128,512]{1,0:T(8,128)S(1)}, f32[128,512]{1,0:T(8,128)}, u32[]{:S(2)}) copy-start(f32[128,512]{1,0:T(8,128)} %get-tuple-element.34) | copy-start | bytes 786436

commit v2 on v1

--- a/solution.py
+++ b/solution.py
@@ -46,6 +46,7 @@
     dwu,
     dwd,
     sel,
+    sw,
     send,
     xc,
     ga,
@@ -82,10 +83,14 @@
     py_r,
     ret_s,
     ret_r,
-    mt_s,
-    mt_r,
+    mtc_s,
+    mtc_r,
+    mty_s,
+    mty_r,
     mr_s,
     mr_r,
+    mrc_s,
+    mrc_r,
     c_s,
     c_r,
 ):
@@ -100,6 +105,7 @@
     rows = half * cap
     slots = n_sp * cap
     peer = (i, y * 2 + 1 - c)
+    straight = ()
 
     def columns(g):
         return pl.ds(pl.multiple_of(g * dg, dg), dg)
@@ -147,17 +153,18 @@
     place = dot(named.astype(BF16), jnp.where(earlier, 1.0, 0.0).astype(BF16), 1, 0)
     place = jnp.where(named > 0.5, place, -1.0).astype(jnp.int32)
     slot_iota = lax.broadcasted_iota(jnp.int32, (cap, tok), 0)
-    mix_part = mix[:, columns(t)]
-    og_part = og[:, columns(t)]
     for e in range(n_sp):
         here = jnp.where(place[e : e + 1, :] == slot_iota, 1.0, 0.0)
         slot_weight = jnp.sum(here * weight[e : e + 1, :], axis=1, keepdims=True)
-        here = here.astype(BF16)
-        sel[e * cap : (e + 1) * cap, :] = here
-        send[0, e] = dot(here, mix_part, 1, 0).astype(BF16)
-        send[1, e] = (dot(here, og_part, 1, 0) * slot_weight).astype(BF16)
-
-    ga[i] = (gb[...].astype(F32) * st[...]).astype(BF16)
+        sel[e * cap : (e + 1) * cap, :] = here.astype(BF16)
+        sw[e * cap : (e + 1) * cap, :] = jnp.broadcast_to(slot_weight, (cap, sw.shape[1]))
+    chosen = sel[...]
+    for q in range(ny):
+        cols = columns(2 * y_up(q) + c)
+        send[0, q] = dot(chosen, mix[:, cols], 1, 0).astype(BF16).reshape(n_sp, cap, dg)
+        send[1, q] = (
+            (dot(chosen, og[:, cols], 1, 0) * sw[:, 0:1]).astype(BF16).reshape(n_sp, cap, dg)
+        )
     pl.semaphore_wait(barrier, n_sp + n_tp - 2)
 
     pending = []
@@ -166,22 +173,35 @@
         copy.start()
         pending.append(copy)
 
-    own = pltpu.make_async_copy(send.at[:, i], xc.at[:, t, i], l_sem.at[0])
-    own.start()
-
-    def dispatch(k):
+    def groups(k):
+        return range(ny) if k in straight else range(1)
+
+    def dispatch(q, k):
         return remote(
-            send.at[:, later(k)], xc.at[:, t, i], sp_s.at[k], sp_r.at[k], (later(k), t)
-        )
-
-    for k in range(1, n_sp):
-        go(dispatch(k))
+            send.at[:, q, later(k)],
+            xc.at[:, 2 * y_up(q) + c, i],
+            sp_s.at[q, k],
+            sp_r.at[q, k],
+            (later(k), t),
+        )
+
+    for k in range(1, n_sp):
+        for q in groups(k):
+            go(dispatch(q, k))
     go(
         remote(
             st.at[pl.ds(tok - 8, 8)], pv, pv_sem.at[0], pv_sem.at[1], (later(1), t)
         )
     )
     pv_copy = pending[-1]
+
+    mine = pl.ds(pl.multiple_of(i * cap, cap), cap)
+    here, slot_weight = sel[mine, :], sw[mine, 0:1]
+    for g in range(n_tp):
+        cols = slice(g * dg, (g + 1) * dg)
+        xc[0, g, i] = dot(here, mix[:, cols], 1, 0).astype(BF16)
+        xc[1, g, i] = (dot(here, og[:, cols], 1, 0) * slot_weight).astype(BF16)
+    ga[i] = (gb[...].astype(F32) * st[...]).astype(BF16)
 
     def to_core(q, k):
         block = xc.at[:, 2 * y_up(q) + c, before(k)]
@@ -197,9 +217,13 @@
         block = xc.at[:, 2 * y_up(ny - q) + c, before(k)]
         return remote(block, block, y_s.at[q, k], y_r.at[q, k], (i, 2 * y_up(q) + c))
 
-    def from_sp(k):
+    def from_sp(q, k):
         return remote(
-            send.at[:, later(k)], xc.at[:, t, before(k)], sp_s.at[k], sp_r.at[k], (later(k), t)
+            send.at[:, q, later(k)],
+            xc.at[:, 2 * y_up(q) + c, before(k)],
+            sp_s.at[q, k],
+            sp_r.at[q, k],
+            (later(k), t),
         )
 
     def from_core(q, k):
@@ -207,15 +231,17 @@
         return remote(block, block, core_s.at[q, k], core_r.at[q, k], peer)
 
     def spread(k):
-        if k == 0:
-            own.wait()
-        else:
-            from_sp(k).wait_recv()
-        for q in range(1, ny):
-            go(to_y(q, k))
-        go(to_core(0, k))
+        for q in groups(k):
+            from_sp(q, k).wait_recv()
+        if k not in straight:
+            for q in range(1, ny):
+                go(to_y(q, k))
+        for q in groups(k):
+            go(to_core(q, k))
 
     def hand_on(k):
+        if k in straight:
+            return
         for q in range(1, ny):
             from_y(q, k).wait_recv()
             go(to_core(ny - q, k))
@@ -303,27 +329,41 @@
         copy.start()
         return copy
 
-    for k in range(n_sp):
+    for k in range(1, n_sp):
         spread(k)
-        if k >= 1:
+        if 1 < k <= half:
             hand_on(k - 1)
-    hand_on(n_sp - 1)
+
+    pair_peer = (i + 1 - 2 * (i % 2), t)
 
     def share_gated(k):
         return remote(ga.at[i], ga.at[i], ga_s.at[k], ga_r.at[k], (later(k), t))
 
-    for k in range(1, n_sp):
+    def get_gated(k):
+        return remote(ga.at[i], ga.at[before(k)], ga_s.at[k], ga_r.at[k], (later(k), t))
+
+    def pass_gated(k):
+        block = ga.at[before(k)]
+        return remote(block, block, ga_s.at[k + 1], ga_r.at[k + 1], pair_peer)
+
+    def passed_gated(k):
+        block = ga.at[lax.rem(pair_peer[0] + n_sp - k, n_sp)]
+        return remote(block, block, ga_s.at[k + 1], ga_r.at[k + 1], pair_peer)
+
+    for k in range(2, n_sp, 2):
         go(share_gated(k))
     for load in loads:
         load.wait()
 
     def arrived(m):
-        for k in range(m * half, (m + 1) * half):
+        for k in range(max(1, m * half), (m + 1) * half):
             for q in range(ny):
                 from_core(q, k).wait_recv()
 
     arrived(0)
     grads = expert(0)
+    for k in range(half, n_sp):
+        hand_on(k)
     partials(0, grads)
     arrived(1)
     grads = expert(1)
@@ -335,6 +375,10 @@
     outs.append(weight_grad(ug, 0, dwu, dwu_h, 1))
     fold_y(1)
     outs.append(weight_grad(hid, 1, dwd, dwd_h, 2))
+    for k in range(0, n_sp, 2):
+        if k:
+            get_gated(k).wait_recv()
+        go(pass_gated(k))
 
     pltpu.make_async_copy(fb.at[0, pl.ds(0, cap)], ret.at[i], l_sem.at[1]).wait()
 
@@ -354,39 +398,62 @@
     mid = (og[:, columns(t)].astype(F32).T + routed).astype(BF16)
     mt[t] = mid
 
-    def share_mid(k):
-        return remote(mt.at[t], mt.at[t], mt_s.at[k], mt_r.at[k], (i, lax.rem(t + k, n_tp)))
-
-    def get_mid(k):
-        block = mt.at[lax.rem(t + n_tp - k, n_tp)]
-        return remote(block, block, mt_s.at[k], mt_r.at[k], (i, lax.rem(t + k, n_tp)))
-
-    for k in range(1, n_tp):
-        go(share_mid(k))
+    def mid_core(q):
+        block = mt.at[2 * y_up(q) + c]
+        return remote(block, block, mtc_s.at[q], mtc_r.at[q], peer)
+
+    def mid_from_core(q):
+        block = mt.at[2 * y_up(q) + 1 - c]
+        return remote(block, block, mtc_s.at[q], mtc_r.at[q], peer)
+
+    def mid_y(q):
+        return remote(mt.at[t], mt.at[t], mty_s.at[q], mty_r.at[q], (i, 2 * y_up(q) + c))
+
+    def mid_from_y(q):
+        block = mt.at[2 * y_up(ny - q) + c]
+        return remote(block, block, mty_s.at[q], mty_r.at[q], (i, 2 * y_up(q) + c))
+
+    for q in range(1, ny):
+        go(mid_y(q))
+    go(mid_core(0))
 
     row = lax.broadcasted_iota(jnp.int32, dc.shape, 0)
     decay = dc[...]
     head = decay[0:1, :]
     factor = jnp.where(row < tok - 1, pltpu.roll(decay, tok - 1, 0), 1.0)
-    for k in range(1, n_tp):
-        get_mid(k).wait_recv()
-
-    share = mr.shape[1]
+    for q in range(1, ny):
+        mid_from_y(q).wait_recv()
+        go(mid_core(ny - q))
+    for q in range(ny):
+        mid_from_core(q).wait_recv()
+
+    share = 2 * mr.shape[2]
     per = dg // share if dg >= share else 1
 
-    def rows_for(s):
-        return mt.at[s // per, pl.ds(pl.multiple_of((s % per) * share, share), share)]
+    part = share // 2
+
+    def rows_for(s, h):
+        first = (s % per) * share + h * part
+        return mt.at[s // per, pl.ds(pl.multiple_of(first, part), part)]
 
     def share_rows(k):
-        return remote(rows_for(later(k)), mr.at[i], mr_s.at[k], mr_r.at[k], (later(k), t))
+        return remote(rows_for(later(k), c), mr.at[i, c], mr_s.at[k], mr_r.at[k], (later(k), t))
 
     def get_rows(k):
-        return remote(rows_for(later(k)), mr.at[before(k)], mr_s.at[k], mr_r.at[k], (later(k), t))
+        return remote(
+            rows_for(later(k), c), mr.at[before(k), c], mr_s.at[k], mr_r.at[k], (later(k), t)
+        )
+
+    def swap_rows(k, h):
+        block = mr.at[before(k), h]
+        return remote(block, block, mrc_s.at[k], mrc_r.at[k], peer)
 
     for k in range(1, n_sp):
         go(share_rows(k))
-    own_rows = pltpu.make_async_copy(rows_for(i), mr.at[i], l_sem.at[2])
-    own_rows.start()
+    for h in range(2):
+        own_rows = pltpu.make_async_copy(rows_for(i, h), mr.at[i, h], l_sem.at[h])
+        own_rows.start()
+        own_rows.wait()
 
     act = dot(mt[...].reshape(n_tp * dg, tok), wp[...], 0, 0)
     grad = act * gb[...].astype(F32)
@@ -411,15 +478,17 @@
     for k in range(1, n_sp):
         go(share_carry(k))
 
-    own_rows.wait()
-    for k in range(1, n_sp):
-        remote(ga.at[i], ga.at[before(k)], ga_s.at[k], ga_r.at[k], (later(k), t)).wait_recv()
+    for k in range(1, n_sp):
+        get_rows(k).wait_recv()
+        go(swap_rows(k, c))
+    for k in range(0, n_sp, 2):
+        passed_gated(k).wait_recv()
     total = None
     for k in range(n_sp):
         if k:
-            get_rows(k).wait_recv()
+            swap_rows(k, 1 - c).wait_recv()
         src = before(k)
-        term = dot(mr[src], ga[src], 1, 0)
+        term = dot(mr[src].reshape(share, tok), ga[src], 1, 0)
         total = term if total is None else total + term
     gproj[...] = total
 
@@ -440,6 +509,30 @@
         copy.wait()
     for copy in pending:
         copy.wait_send()
+
+
+def settle(count, *refs):
+    ins, outs, held = refs[:count], refs[count : 2 * count], refs[2 * count : 3 * count]
+    in_sem, out_sem = refs[3 * count :]
+    jobs = []
+    for n in range(count):
+        pieces = 2 if n < 3 else 1
+        rows = ins[n].shape[0] // pieces
+        for p in range(pieces):
+            part = pl.ds(p * rows, rows)
+            jobs.append(
+                (
+                    pltpu.make_async_copy(ins[n].at[part], held[n].at[part], in_sem.at[n, p]),
+                    pltpu.make_async_copy(held[n].at[part], outs[n].at[part], out_sem.at[n, p]),
+                )
+            )
+    for bring, _ in jobs:
+        bring.start()
+    for bring, put in jobs:
+        bring.wait()
+        put.start()
+    for _, put in jobs:
+        put.wait()
 
 
 def local(
@@ -485,7 +578,8 @@
             pltpu.VMEM((width, channels), BF16),
             *([pltpu.VMEM(weight, BF16)] * 6),
             pltpu.VMEM((n_sp * cap, tok), BF16),
-            pltpu.VMEM((2, n_sp, cap, dg), BF16),
+            pltpu.VMEM((n_sp * cap, 128), F32),
+            pltpu.VMEM((2, ny, n_sp, cap, dg), BF16),
             pltpu.VMEM((2, n_tp, n_sp, cap, dg), BF16),
             pltpu.VMEM((n_sp, tok, channels), BF16),
             pltpu.VMEM((8, channels), F32),
@@ -494,24 +588,21 @@
             pltpu.VMEM((CHUNKS, half_rows, dg), BF16),
             pltpu.VMEM((n_sp, cap, dg), BF16),
             pltpu.VMEM((n_tp, dg, tok), BF16),
-            pltpu.VMEM((n_sp, share, tok), BF16),
+            pltpu.VMEM((n_sp, 2, share // 2, tok), BF16),
             pltpu.VMEM((8, channels), F32),
             pltpu.VMEM((n_sp, 8, channels), F32),
             dma((4,)),
             dma((3,)),
             dma((3,)),
-            dma((n_sp,)),
-            dma((n_sp,)),
-            *([dma((ny, n_sp))] * 4),
+            *([dma((ny, n_sp))] * 6),
             dma((n_sp,)),
             dma((n_sp,)),
             dma((2,)),
             *([dma((CHUNKS, ny))] * 4),
             dma((n_sp,)),
             dma((n_sp,)),
-            dma((n_tp,)),
-            dma((n_tp,)),
-            *([dma((n_sp,))] * 4),
+            *([dma((ny,))] * 4),
+            *([dma((n_sp,))] * 6),
         ],
         compiler_params=pltpu.CompilerParams(
             collective_id=0, has_side_effects=True, vmem_limit_bytes=60 * 1024 * 1024
@@ -529,6 +620,18 @@
         w_up[0],
         w_down[0],
     )
+    count = len(outs)
+    outs = pl.pallas_call(
+        functools.partial(settle, count),
+        out_shape=[jax.ShapeDtypeStruct(o.shape, o.dtype) for o in outs],
+        in_specs=[hbm] * count,
+        out_specs=[hbm] * count,
+        scratch_shapes=[
+            *(pltpu.VMEM(o.shape, o.dtype) for o in outs),
+            dma((count, 2)),
+            dma((count, 2)),
+        ],
+    )(*outs)
     return (outs[0][None], outs[1][None], outs[2][None], *outs[3:])
 
 

time: 106 us -> 91.7 us (0.87)
  local copies, waits for them, and re-layouts: 9.86 us -> 0 us
  Pallas kernels: 95.6 us -> 90.6 us
    pallas_call x1, Pallas kernels: 95.6 us -> 84.6 us  [local(): pl.pallas_call(functools.partial(kernel, n_sp, n_tp), out_shape=[jax.Shap...]
    unnamed x19 -> x0, local copies, waits for them, and re-layouts: 9.86 us -> none
    pallas_call x0 -> x1, Pallas kernels: none -> 6.03 us  [local(): pl.pallas_call(functools.partial(settle, count), out_shape=[jax.ShapeDtyp...]
where the time goes in v2:
time: 91.7 us; the launch traced here: 91.3 us
  Pallas kernels  90.6 us (99%)
    pallas_call x1, Pallas kernels, local(): pl.pallas_call(functools.partial(kernel, n_sp, n_tp), out_shape=[jax.Shap...  84.6 us
    pallas_call x1, Pallas kernels, local(): pl.pallas_call(functools.partial(settle, count), out_shape=[jax.ShapeDtyp...  6.03 us

profile of v2, /device:TPU:0, one launch (start us, length us, event | category | flops | bytes accessed | tf_op | source)
XLA Modules:
  0.0 91.3 jit_solution(13950462829740153176)
XLA Ops:
  0.6 84.6 %shard_map.162 = (bf16[512,2048]{1,0:T(8,128)(2,1)}, bf16[512,2048]{1,0:T(8,128)(2,1)}, bf16[512,2048]{1,0:T(8,128)(2,1)}, f32[256,512]{1,0:T(8,128)}, bf16[128,...) custom-call(s32[2,128]{1,0:T(2,128)} %bitcast.11, f32[2,128]{1,0:T(2,128)} %bitcast.12, ...), custom_call_target="tpu_custom_call" | custom-call | tf_op jit(solution)/shard_map/pallas_call | solution.py:566
  85.2 6.0 %shard_map.163 = (bf16[512,2048]{1,0:T(8,128)(2,1)}, bf16[512,2048]{1,0:T(8,128)(2,1)}, bf16[512,2048]{1,0:T(8,128)(2,1)}, f32[256,512]{1,0:T(8,128)}, bf16[128,...) custom-call(bf16[512,2048]{1,0:T(8,128)(2,1)} %get-tuple-element.21.refs_0_, ...), custom_call_target="tpu_custom_call" | custom-call | tf_op jit(solution)/shard_map/pallas_call | solution.py:624
